TPU v7x, 32 devices: a whole 2x2x4 slice. The times are simulated.
32 devices in a mesh: ep: 8 (over z, core), tp: 4 (over y, x).
Axes of the slice: x: 2, y: 2, z: 4, core: 2. Of those that a mesh axis runs over, the one named last changes fastest.
Arguments:
- query_vectors: bfloat16 [4096, 4096], P('ep', 'tp'), may hold values from -6 to 6
- key_vectors: bfloat16 [4096, 2048], P('ep', 'tp'), may hold values from -6 to 6
- value_vectors: bfloat16 [4096, 2048], P('ep', 'tp'), may hold values from -64 to 64
- query_gain: float32 [128], replicated, may hold values from 0.1 to 1.9
- key_gain: float32 [128], replicated, may hold values from 0.1 to 1.9
- sink_logits: float32 [32], P('tp'), may hold values from 3 to 7
- moe_rows: bfloat16 [1280, 4096], P('ep', 'tp'), may hold values from -6 to 6
- norm_gain: float32 [4096], replicated, may hold values from 0.1 to 1.9
- expert_ids: int32 [1280, 4], P('ep'), may hold values from 0 to 7, all different within a row; in each aligned block of 160 rows (0 to 159, 160 to 319, ...) at most 120 rows name the same one
- route_weights: float32 [1280, 4], P('ep'), may hold values from 0.25 to 2.5
- expert_gate: bfloat16 [8, 4096, 2048], P('ep', None, 'tp'), may hold values from -0.09375 to 0.09375
- expert_up: bfloat16 [8, 4096, 2048], P('ep', None, 'tp'), may hold values from -0.09375 to 0.09375
- expert_down: bfloat16 [8, 2048, 4096], P('ep', None, 'tp'), may hold values from -0.125 to 0.125
- shared_gate: bfloat16 [4096, 512], P(None, 'tp'), may hold values from -0.09375 to 0.09375
- shared_up: bfloat16 [4096, 512], P(None, 'tp'), may hold values from -0.09375 to 0.09375
- shared_down: bfloat16 [512, 4096], P(None, 'tp'), may hold values from -0.25 to 0.25
Outputs:
- attended: bfloat16 [4096, 4096], P('ep', 'tp')
- moe_out: bfloat16 [1280, 4096], P('ep', 'tp')
Inputs may be any that keep to these rules, and one draw needn't show every extreme that they name: `expert_ids`: each row names 4 different experts. Within the rows of one index of ep (aligned blocks of 160 rows), no expert is named by more than 120 rows, and in some block one expert is named by exactly 120.
All inputs are finite; a program needn't handle non-finite values.
Results may differ from a plain program's by a relative error of at most 0.0071.
Values may be sent and summed in bfloat16 or wider, within the bound.
A program may use at most 128 MiB of HBM per device.

v0:
```python
import jax
import jax.numpy as jnp
from jax import lax
from jax.sharding import PartitionSpec as P

HEAD_DIM = 128
WINDOW = 128
GRID_W = 64
D = 4096
TOP_K = 4
epsilon = 1e-06
rotary_base = 10000.0


def padded_2(block, sides, width):
    for axis, dim in sides:
        count = lax.axis_size(axis)
        forward = [(i, i + 1) for i in range(count - 1)]
        backward = [(target, source) for source, target in forward]
        low = lax.ppermute(
            lax.slice_in_dim(block, block.shape[dim] - width, None, axis=dim), axis, forward
        )
        high = lax.ppermute(lax.slice_in_dim(block, 0, width, axis=dim), axis, backward)
        block = jnp.concatenate([low, block, high], axis=dim)
    return block


def half_turn(halves):
    leading, trailing = jnp.split(halves, 2, axis=-1)
    return jnp.concatenate([-trailing, leading], axis=-1)


def rotate_heads(vectors, head_gain, positions):
    floats = vectors.astype(jnp.float32)
    normed = (
        floats * lax.rsqrt(jnp.mean(floats * floats, axis=-1, keepdims=True) + epsilon) * head_gain
    )
    quarter = HEAD_DIM // 4
    freq_index = jnp.arange(quarter, dtype=jnp.int32).astype(jnp.float32)
    inverse = rotary_base ** (-4.0 * freq_index / HEAD_DIM)
    grid_row = (positions // GRID_W).astype(jnp.float32)[:, None] * inverse
    grid_col = (positions % GRID_W).astype(jnp.float32)[:, None] * inverse
    angles = jnp.concatenate([grid_row, grid_row, grid_col, grid_col], axis=-1)[:, None, :]
    row_half, col_half = jnp.split(normed, 2, axis=-1)
    turned = jnp.concatenate([half_turn(row_half), half_turn(col_half)], axis=-1)
    return (normed * jnp.cos(angles) + turned * jnp.sin(angles)).astype(jnp.bfloat16)


def attend_window(query_vectors, key_vectors, value_vectors, query_gain, key_gain, sink_logits):
    length = query_vectors.shape[0]
    heads_here = sink_logits.shape[0]
    kv_here = key_vectors.shape[1] // HEAD_DIM
    grouping = heads_here // kv_here
    shard_start = lax.axis_index("ep") * length
    positions = shard_start + jnp.arange(length, dtype=jnp.int32)
    queries = rotate_heads(
        query_vectors.reshape(length, heads_here, HEAD_DIM), query_gain, positions
    )
    turned_keys = rotate_heads(key_vectors.reshape(length, kv_here, HEAD_DIM), key_gain, positions)
    turned_keys = turned_keys.reshape(length, kv_here * HEAD_DIM)
    padded = padded_2(jnp.stack([turned_keys, value_vectors]), (("ep", 1),), WINDOW)
    extent = length + 2 * WINDOW
    near_keys = padded[0].reshape(extent, kv_here, HEAD_DIM)
    near_values = padded[1].reshape(extent, kv_here, HEAD_DIM)
    key_pos = shard_start - WINDOW + jnp.arange(extent, dtype=jnp.int32)
    inside = (
        (jnp.abs(positions[:, None] - key_pos[None, :]) <= WINDOW)
        & (key_pos >= 0)[None, :]
        & (key_pos < lax.axis_size("ep") * length)[None, :]
    )
    scores = jnp.einsum(
        "qhgd,khd->hgqk",
        queries.reshape(length, kv_here, grouping, HEAD_DIM),
        near_keys,
        preferred_element_type=jnp.float32,
    ) * HEAD_DIM ** (-0.5)
    raised = jnp.where(inside, jnp.exp(scores), 0.0)
    denominator = jnp.exp(sink_logits).reshape(kv_here, grouping)[:, :, None] + jnp.sum(
        raised, axis=-1
    )
    weights = (raised / denominator[..., None]).astype(jnp.bfloat16)
    mixed = jnp.einsum("hgqk,khd->qhgd", weights, near_values, preferred_element_type=jnp.float32)
    return mixed.astype(jnp.bfloat16).reshape(length, heads_here * HEAD_DIM)


def project(block_rows, gain_piece, gate_rows, up_rows):
    floats = block_rows.astype(jnp.float32)
    weighted = (floats * gain_piece).astype(jnp.bfloat16)
    gate_sum = jnp.dot(weighted, gate_rows, preferred_element_type=jnp.float32)
    up_sum = jnp.dot(weighted, up_rows, preferred_element_type=jnp.float32)
    return (gate_sum, up_sum, jnp.sum(floats * floats, axis=1))


def activate(gate_sum, up_sum, squares):
    factor = lax.rsqrt(squares / D + epsilon)[:, None]
    return (jax.nn.silu(gate_sum * factor) * (up_sum * factor)).astype(jnp.bfloat16)


def shards(
    query_vectors,
    key_vectors,
    value_vectors,
    query_gain,
    key_gain,
    sink_logits,
    moe_rows,
    norm_gain,
    expert_ids,
    route_weights,
    expert_gate,
    expert_up,
    expert_down,
    shared_gate,
    shared_up,
    shared_down,
):
    attended = attend_window(
        query_vectors, key_vectors, value_vectors, query_gain, key_gain, sink_logits
    )
    ep_size = lax.axis_size("ep")
    tokens_here, width_here = moe_rows.shape
    capacity = max(2, 3 * tokens_here * TOP_K // (2 * ep_size))
    slots_all = ep_size * capacity
    flat_ids = expert_ids.reshape(-1)
    onehot = (flat_ids[:, None] == jnp.arange(ep_size, dtype=jnp.int32)[None, :]).astype(jnp.int32)
    slot_index = jnp.sum((jnp.cumsum(onehot, axis=0) - onehot) * onehot, axis=1)
    target = flat_ids * capacity + slot_index
    matches = target[None, :] == jnp.arange(slots_all, dtype=jnp.int32)[:, None]
    present = jnp.any(matches, axis=1)
    owner_row = jnp.arange(tokens_here * TOP_K, dtype=jnp.int32) // TOP_K
    source_row = jnp.sum(jnp.where(matches, owner_row[None, :], 0), axis=1)
    local_gate = expert_gate[0]
    local_up = expert_up[0]
    local_down = expert_down[0]
    units_here = local_gate.shape[1]
    shared_units = shared_gate.shape[1]
    outgoing = jnp.where(
        present[:, None], jnp.take(moe_rows, source_row, axis=0), jnp.zeros((), jnp.bfloat16)
    )
    arrived = lax.all_to_all(
        outgoing.reshape(ep_size, capacity, width_here),
        "ep",
        split_axis=0,
        concat_axis=0,
        tiled=True,
    )
    arrived = arrived.reshape(slots_all, width_here)
    routed = project(
        lax.all_gather(arrived, "tp", axis=1, tiled=True), norm_gain, local_gate, local_up
    )
    shared = project(
        lax.all_gather(moe_rows, "tp", axis=1, tiled=True), norm_gain, shared_gate, shared_up
    )
    gate_sum, up_sum, squares, shared_gsum, shared_usum, own_squares = tuple(
        (new_term for new_term in routed + shared)
    )
    hidden = activate(gate_sum, up_sum, squares)
    shared_hidden = activate(shared_gsum, shared_usum, own_squares)
    packing = units_here // shared_units
    stacked = jnp.concatenate(
        [hidden, shared_hidden.reshape(tokens_here // packing, units_here)], axis=0
    )
    columns = local_down.shape[1]
    portion = lax.all_gather(stacked, "tp", axis=1, tiled=True)
    shards_in = portion.shape[1] // units_here
    routed = jnp.dot(portion[:slots_all], local_down, preferred_element_type=jnp.float32)
    shared_piece = portion[slots_all:].reshape(
        tokens_here // packing, shards_in, packing, shared_units
    )
    shared_piece = shared_piece.transpose(0, 2, 1, 3).reshape(tokens_here, shards_in * shared_units)
    shared = jnp.dot(shared_piece, shared_down, preferred_element_type=jnp.float32)
    returned = lax.all_to_all(
        routed.astype(jnp.bfloat16).reshape(ep_size, capacity, columns),
        "ep",
        split_axis=0,
        concat_axis=0,
        tiled=True,
    )
    returned = returned.reshape(slots_all, columns)
    picked = jnp.take(returned, target, axis=0).reshape(tokens_here, TOP_K, columns)
    combined = shared + jnp.sum(route_weights[:, :, None] * picked.astype(jnp.float32), axis=1)
    return (attended, combined.astype(jnp.bfloat16))


def solution(mesh):
    placed = (
        P("ep", "tp"),
        P("ep", "tp"),
        P("ep", "tp"),
        P(),
        P(),
        P("tp"),
        P("ep", "tp"),
        P(),
        P("ep", None),
        P("ep", None),
        P("ep", None, "tp"),
        P("ep", None, "tp"),
        P("ep", None, "tp"),
        P(None, "tp"),
        P(None, "tp"),
        P(None, "tp"),
    )
    return jax.shard_map(
        shards,
        mesh=mesh,
        in_specs=placed,
        out_specs=(P("ep", "tp"), P("ep", "tp")),
        check_vma=False,
    )
```

profile of v0, /device:TPU:0, one launch (start us, length us, event | category | flops | bytes accessed | tf_op | source)
XLA Modules:
  0.0 298.6 jit_solution(4147302405466254535)
XLA Ops:
  7.2 0.9 copy.83
  8.3 1.4 reduce-window.6
  11.2 4.2 %gather_fusion = bf16[960,1024]{1,0:T(8,128)(2,1)S(1)} fusion(bf16[160,1024]{1,0:T(8,128)(2,1)S(1)} %copy-done.1, s32[1024]{0:T(1024)S(1)} %pad_clamp_fusion.1), kind=kCustom, calls=%fused_computation | custom fusion | bytes 3936000 | tf_op jit(solution)/shard_map/jit(_take)/gather | solution.py:138
  15.4 1.5 select_select_fusion
  16.9 6.4 %all-to-all-start = ((bf16[8,120,1024]{2,1,0:T(8,128)(2,1)}), bf16[8,120,1024]{2,1,0:T(8,128)(2,1)S(1)}, u32[]{:S(2)}, u32[]{:S(2)}) async-start(bf16[8,120,1024]{2,1,0:T(8,128)(2,1)} %select_select_fusion), calls=%async_computation | async-start | bytes 3932160 | tf_op jit(solution)/shard_map/all_to_all | solution.py:140
  23.3 0.7 all-gather.6.cloned.1.call-update
  24.0 45.4 %all-to-all-done = bf16[8,120,1024]{2,1,0:T(8,128)(2,1)S(1)} async-done(((bf16[8,120,1024]{2,1,0:T(8,128)(2,1)}), bf16[8,120,1024]{2,1,0:T(8,128)(2,1)S(1)}, u32[]{:S(2)}, u32[]{:S(2)}) %all-to-all-start) | async-done | bytes 1966112 | tf_op jit(solution)/shard_map/all_to_all | solution.py:140
  69.5 1.3 copy-done.6
  70.9 1.8 fusion.14
  72.8 2.1 fusion.37
  74.9 0.5 fusion.46
  75.4 77.6 %all-gather.4.cloned.1.call-done = bf16[960,4096]{1,0:T(8,128)(2,1)} async-done(((bf16[960,1024]{1,0:T(8,128)(2,1)}), bf16[960,4096]{1,0:T(8,128)(2,1)}) %all-gather.4.cloned.1.call-update) | async-done | bytes 7864336 | tf_op jit(solution)/shard_map/all_gather | solution.py:149
  153.1 5.0 %fusion.1 = f32[960]{0:T(1024)S(1)} fusion(bf16[960,4096]{1,0:T(8,128)(2,1)} %all-gather.4.cloned.1.call-done), kind=kLoop, calls=%fused_computation.5 | loop fusion | flops 11795520 | bytes 7868160 | tf_op jit(solution)/shard_map/reduce_sum | solution.py:91
  158.0 0.5 copy-done.5
  158.5 6.4 %fusion.3 = f32[960,512]{1,0:T(8,128)S(1)} fusion(bf16[960,4096]{1,0:T(8,128)(2,1)S(1)} %copy-done.5, f32[4096]{0:T(1024)S(1)} %copy-done.27, bf16[1,4096,512]{2,1,0:T(8,128)(2,1)} %param.27), kind=kOutput, calls=%fused_computation.9 | convolution fusion | flops 4038328320 | bytes 14041088 | tf_op jit(solution)/shard_map/dot_general | solution.py:90
  165.0 4.6 %multiply_convert_fusion = bf16[960,512]{1,0:T(8,128)(2,1)S(1)} fusion(f32[960,512]{1,0:T(8,128)S(1)} %fusion.3, bf16[1,4096,512]{2,1,0:T(8,128)(2,1)S(1)} %copy-done.25, bf16[960,4096]{1,0:T(8,128)(2,1)S(1)} %copy-done.5, f32[4096]{0:T(1024)S(1)} %copy-done.27, f32[960]{0:T(1024)S(1)} %add_rsqrt_fusion.2), kind=kOutput, calls=%fused_computation.33 | convolution fusion | flops 4042260480 | bytes 15027968 | tf_op jit(solution)/shard_map/dot_general | solution.py:89
  169.6 1.0 pad_maximum_fusion.1
  171.6 1.2 fusion.60
  174.1 1.0 pad_maximum_fusion.3
  175.1 1.3 collective-permute-start.1
  176.4 3.7 %collective-permute-start = (bf16[2,128,512]{1,2,0:T(8,128)(2,1)}, bf16[2,128,512]{1,2,0:T(8,128)(2,1)}, u32[]{:S(2)}, u32[]{:S(2)}) collective-permute-start(bf16[2,128,512]{1,2,0:T(8,128)(2,1)} %get-tuple-element.18), channel_id=1, source_target_pairs={{0,4},{4,8},{8,12},{12,16},{16,20},{20,24},{24,28},{1,5},{5,9},{9,... | collective-permute-start | bytes 786440 | tf_op jit(solution)/shard_map/ppermute | solution.py:20
  180.1 1.5 copy.75
  181.6 4.2 %reshape.381 = f32[512,4,2,128]{3,2,1,0:T(2,128)} reshape(bf16[512,1024]{1,0:T(8,128)(2,1)} %param.16) | data formatting | bytes 3145728 | tf_op jit(solution)/shard_map/convert_element_type | solution.py:34
  186.2 0.5 multiply_multiply_fusion
  187.0 2.0 copy.80
  189.0 1.9 copy.79
  190.9 1.9 copy.78
  192.8 1.9 copy.77
  194.8 0.6 add.209
  195.7 0.8 copy.88
  196.5 0.7 copy.90
  197.3 0.6 fusion.69
  197.9 1.4 fusion.30
  199.3 23.1 %all-gather.8.cloned.1.call-done = bf16[1000,2048]{1,0:T(8,128)(2,1)} async-done(((bf16[1000,512]{1,0:T(8,128)(2,1)}), bf16[1000,2048]{1,0:T(8,128)(2,1)}) %all-gather.8.cloned.1.call-update) | async-done | bytes 4096016 | tf_op jit(solution)/shard_map/all_gather | solution.py:164
  222.4 8.9 %fusion.20 = bf16[960,1024]{1,0:T(8,128)(2,1)} fusion(bf16[1,2048,1024]{2,1,0:T(8,128)(2,1)} %param.28, bf16[1000,2048]{1,0:T(8,128)(2,1)} %all-gather.8.cloned.1.call-done), kind=kOutput, calls=%fused_computation.35 | convolution fusion | flops 4027514880 | bytes 10092544 | tf_op jit(solution)/shard_map/dot_general | solution.py:166
  231.3 4.7 %all-to-all-start.1 = ((bf16[8,120,1024]{2,1,0:T(8,128)(2,1)}), bf16[8,120,1024]{2,1,0:T(8,128)(2,1)S(1)}, u32[]{:S(2)}, u32[]{:S(2)}) async-start(bf16[8,120,1024]{2,1,0:T(8,128)(2,1)} %bitcast.104), calls=%async_computation.1 | async-start | bytes 3932160 | tf_op jit(solution)/shard_map/all_to_all | solution.py:172
  236.0 1.3 pad_clamp_fusion
  237.3 1.5 pad_maximum_fusion
  239.2 0.6 copy-done.4
  239.8 0.9 copy-done.2
  240.7 7.2 %fusion.2 = (f32[4,2,512]{2,1,0:T(2,128)S(1)}, f32[4,768,512,2]{2,1,3,0:T(8,128)S(1)}) fusion(pred[512,768]{0,1:T(8,128)(4,1)} %fusion.30, bf16[768,4,128,1]{0,2,3,1:T(8,128)(2,1)S(1)} %bitcast.99, f32[512,4,2,32]{3,0,2,1:T(8,128)S(1)} %copy-done.2, f32[512,4,2,32]{3,0,2,1:T(8,128)S(1)} %copy-done.3, f32[512,4,2,32]{3,0,2,1:T(8,128)S(1)} %copy-done.4, ...), kind=kOutput, calls=%fused_computation.8 | convolution fusion | flops 819458048 | bytes 18514432 | tf_op jit(solution)/shard_map/qhgd,khd->hgqk/dot_general | solution.py:71
  248.0 4.2 %fusion.31 = bf16[4,128,2,512]{3,1,2,0:T(8,128)(2,1)} fusion(bf16[768,4,128,1]{0,2,3,1:T(8,128)(2,1)S(1)} %bitcast.106, f32[4,768,512,2]{2,1,3,0:T(8,128)S(1)} %get-tuple-element.29, f32[4,2,512]{2,1,0:T(2,128)S(1)} %broadcast_add_fusion, pred[512,768]{0,1:T(8,128)(4,1)S(1)} %copy-done.12), kind=kOutput, calls=%fused_computation.40 | convolution fusion | flops 818413568 | bytes 14827520 | tf_op jit(solution)/shard_map/hgqk,khd->qhgd/dot_general | solution.py:82
  252.2 2.3 copy.92
  254.7 27.6 %all-to-all-done.1 = bf16[8,120,1024]{2,1,0:T(8,128)(2,1)S(1)} async-done(((bf16[8,120,1024]{2,1,0:T(8,128)(2,1)}), bf16[8,120,1024]{2,1,0:T(8,128)(2,1)S(1)}, u32[]{:S(2)}, u32[]{:S(2)}) %all-to-all-start.1) | async-done | bytes 1966112 | tf_op jit(solution)/shard_map/all_to_all | solution.py:172
  282.2 3.5 %gather_fusion.1 = bf16[640,1024]{1,0:T(8,128)(2,1)} fusion(bf16[960,1024]{1,0:T(8,128)(2,1)S(1)} %bitcast.92, s32[1024]{0:T(1024)S(1)} %copy-done.19), kind=kCustom, calls=%fused_computation.1 | custom fusion | bytes 2624000 | tf_op jit(solution)/shard_map/jit(_take)/gather | solution.py:180
  285.7 2.6 gather.15
  288.4 2.6 multiply_reduce_fusion
  291.0 1.1 fusion.32
  (115 shorter events, 5.7 us)
Async XLA Ops:
  7.2 283.8 %copy-start = (bf16[512,1024]{1,0:T(8,128)(2,1)S(1)}, bf16[512,1024]{1,0:T(8,128)(2,1)}, u32[]{:S(2)}) copy-start(bf16[512,1024]{1,0:T(8,128)(2,1)} %param.31) | copy-start | bytes 3145732
  7.2 4.0 %copy-start.1 = (bf16[160,1024]{1,0:T(8,128)(2,1)S(1)}, bf16[160,1024]{1,0:T(8,128)(2,1)}, u32[]{:S(2)}) copy-start(bf16[160,1024]{1,0:T(8,128)(2,1)} %param.22) | copy-start | bytes 983044
  16.9 52.6 %all-to-all-start = ((bf16[8,120,1024]{2,1,0:T(8,128)(2,1)}), bf16[8,120,1024]{2,1,0:T(8,128)(2,1)S(1)}, u32[]{:S(2)}, u32[]{:S(2)}) async-start(bf16[8,120,1024]{2,1,0:T(8,128)(2,1)} %select_select_fusion), calls=%async_computation | async-start | bytes 3932160 | tf_op jit(solution)/shard_map/all_to_all | solution.py:140
  23.3 49.5 %copy-start.27 = (f32[4096]{0:T(1024)S(1)}, f32[4096]{0:T(1024)}, u32[]{:S(2)}) copy-start(f32[4096]{0:T(1024)} %param.23) | copy-start | bytes 49156
  23.3 47.7 %all-gather.6.cloned.1.call-start = ((), (), s32[]{:S(2)}) async-start(), calls=%async_computation.3 | async-start | bytes 1638400 | tf_op jit(solution)/shard_map/all_gather | solution.py:152
  24.0 129.1 %all-gather.4.cloned.1.call-start = ((), (), s32[]{:S(2)}) async-start(), calls=%async_computation.2 | async-start | bytes 9830400 | tf_op jit(solution)/shard_map/all_gather | solution.py:149
  69.5 1.3 copy-start.6
  70.8 4.0 %copy-start.26 = (bf16[4096,128]{1,0:T(8,128)(2,1)S(1)}, bf16[4096,128]{1,0:T(8,128)(2,1)}, u32[]{:S(2)}) copy-start(bf16[4096,128]{1,0:T(8,128)(2,1)} %param.30) | copy-start | bytes 3145732
  70.9 151.5 %all-gather.8.cloned.1.call-start = ((), (), s32[]{:S(2)}) async-start(), calls=%async_computation.4 | async-start | bytes 5120000 | tf_op jit(solution)/shard_map/all_gather | solution.py:164
  70.9 4.0 %copy-start.13 = (bf16[160,4096]{1,0:T(8,128)(2,1)S(1)}, bf16[160,4096]{1,0:T(8,128)(2,1)}, u32[]{:S(2)}) copy-start(bf16[160,4096]{1,0:T(8,128)(2,1)} %all-gather.6.cloned.1.call-done) | copy-start | bytes 3932164
  153.1 5.5 %copy-start.5 = (bf16[960,4096]{1,0:T(8,128)(2,1)S(1)}, bf16[960,4096]{1,0:T(8,128)(2,1)}, u32[]{:S(2)}) copy-start(bf16[960,4096]{1,0:T(8,128)(2,1)} %all-gather.4.cloned.1.call-done) | copy-start | bytes 23592964
  158.5 6.4 %copy-start.25 = (bf16[1,4096,512]{2,1,0:T(8,128)(2,1)S(1)}, bf16[1,4096,512]{2,1,0:T(8,128)(2,1)}, u32[]{:S(2)}) copy-start(bf16[1,4096,512]{2,1,0:T(8,128)(2,1)} %param.26) | copy-start | bytes 12582916
  169.5 1.2 copy-start.14
  169.6 1.6 copy-start.15
  171.1 3.0 %copy-start.7 = (bf16[512,512]{0,1:T(8,128)(2,1)}, bf16[512,512]{0,1:T(8,128)(2,1)S(1)}, u32[]{:S(2)}) copy-start(bf16[512,512]{0,1:T(8,128)(2,1)S(1)} %copy.74) | copy-start | bytes 1572868
  171.4 1.9 copy-start.24
  172.8 0.7 copy-start.10
  172.8 0.8 copy-start.11
  174.1 2.3 copy-start.9
  175.1 62.2 %collective-permute-start.1 = (bf16[2,128,512]{1,2,0:T(8,128)(2,1)}, bf16[2,128,512]{1,2,0:T(8,128)(2,1)}, u32[]{:S(2)}, u32[]{:S(2)}) collective-permute-start(bf16[2,128,512]{1,2,0:T(8,128)(2,1)} %get-tuple-element.19), channel_id=1, source_target_pairs={{4,0},{8,4},{12,8},{16,12},{20,16},{24,20},{28,24},{5,1},{9,5},{13... | collective-permute-start | bytes 786440 | tf_op jit(solution)/shard_map/ppermute | solution.py:23
  176.4 60.9 %collective-permute-start = (bf16[2,128,512]{1,2,0:T(8,128)(2,1)}, bf16[2,128,512]{1,2,0:T(8,128)(2,1)}, u32[]{:S(2)}, u32[]{:S(2)}) collective-permute-start(bf16[2,128,512]{1,2,0:T(8,128)(2,1)} %get-tuple-element.18), channel_id=1, source_target_pairs={{0,4},{4,8},{8,12},{12,16},{16,20},{20,24},{24,28},{1,5},{5,9},{9,... | collective-permute-start | bytes 786440 | tf_op jit(solution)/shard_map/ppermute | solution.py:20
  181.6 4.6 %copy-start.21 = (f32[128]{0:T(128)S(1)}, f32[128]{0:T(128)}, u32[]{:S(2)}) copy-start(f32[128]{0:T(128)} %param.19) | copy-start | bytes 1540
  190.9 3.9 %copy-start.28 = (f32[8]{0:T(128)S(1)}, f32[8]{0:T(128)}, u32[]{:S(2)}) copy-start(f32[8]{0:T(128)} %param.21) | copy-start | bytes 100
  190.9 4.5 %copy-start.18 = (s32[160,4]{0,1:T(4,128)S(1)}, s32[160,4]{0,1:T(4,128)}, u32[]{:S(2)}) copy-start(s32[160,4]{0,1:T(4,128)} %param.24) | copy-start | bytes 7684
  190.9 4.8 %copy-start.23 = (f32[160,4]{0,1:T(4,128)S(1)}, f32[160,4]{0,1:T(4,128)}, u32[]{:S(2)}) copy-start(f32[160,4]{0,1:T(4,128)} %param.25) | copy-start | bytes 7684
  231.3 6.0 %copy-start.8 = (bf16[512,512]{0,1:T(8,128)(2,1)S(1)}, bf16[512,512]{0,1:T(8,128)(2,1)}, u32[]{:S(2)}) copy-start(bf16[512,512]{0,1:T(8,128)(2,1)} %copy-done.7) | copy-start | bytes 1572868
  231.3 51.0 %all-to-all-start.1 = ((bf16[8,120,1024]{2,1,0:T(8,128)(2,1)}), bf16[8,120,1024]{2,1,0:T(8,128)(2,1)S(1)}, u32[]{:S(2)}, u32[]{:S(2)}) async-start(bf16[8,120,1024]{2,1,0:T(8,128)(2,1)} %bitcast.104), calls=%async_computation.1 | async-start | bytes 3932160 | tf_op jit(solution)/shard_map/all_to_all | solution.py:172
  237.3 1.9 copy-start.3
  237.3 2.5 copy-start.4
  238.8 1.9 copy-start.2
  238.8 1.9 copy-start.22
  240.7 7.2 %copy-start.20 = (f32[4,2]{1,0:T(4,128)S(1)}, f32[4,2]{1,0:T(4,128)}, u32[]{:S(2)}) copy-start(f32[4,2]{1,0:T(4,128)} %add.209) | copy-start | bytes 100
  240.7 7.3 %copy-start.12 = (pred[512,768]{0,1:T(8,128)(4,1)S(1)}, pred[512,768]{0,1:T(8,128)(4,1)}, u32[]{:S(2)}) copy-start(pred[512,768]{0,1:T(8,128)(4,1)} %fusion.30) | copy-start | bytes 1179652
  252.2 2.3 slice-start
  252.2 30.0 %copy-start.19 = (s32[1024]{0:T(1024)S(1)}, s32[1024]{0:T(1024)}, u32[]{:S(2)}) copy-start(s32[1024]{0:T(1024)} %pad_clamp_fusion) | copy-start | bytes 12292
  285.7 2.7 copy-start.16
  285.7 2.7 copy-start.17
Sparse Core Ops, SparseCore 0:
  25.9 30.1 all-gather.5
  71.0 82.0 all-gather.3
  170.7 51.6 all-gather.7
where the time goes:
time: 299 us
  waiting for transfers between devices  174 us (58%)
  local copies, waits for them, and re-layouts  35.3 us (12%)
  matrix products  34.9 us (12%)
  other arithmetic  23.4 us (8%)
  starting transfers between devices  16.2 us (5%)
  between operations  14.3 us (5%)
    all_gather x1, waiting for transfers between devices, shards(): lax.all_gather(arrived, 'tp', axis=1, tiled=True)  77.6 us
    all_to_all x1, waiting for transfers between devices, shards(): lax.all_to_all(outgoing.reshape(ep_size, capacity, width_here), 'ep', spl...  45.4 us
    all_to_all x1, waiting for transfers between devices, shards(): lax.all_to_all(routed.astype(jnp.bfloat16).reshape(ep_size, capacity, col...  27.6 us
    all_gather x1, waiting for transfers between devices, shards(): portion = lax.all_gather(stacked, 'tp', axis=1, tiled=True)  23.1 us
    dot_general x1, matrix products, shards(): jnp.dot(portion[:slots_all], local_down, preferred_element_type=jnp.float32)  8.88 us
    unnamed x63, local copies, waits for them, and re-layouts  8.45 us
    concatenate x4, local copies, waits for them, and re-layouts, rotate_heads(): jnp.concatenate([half_turn(row_half), half_turn(col_half)], axis=-1)  7.81 us
    dot_general x1, matrix products, attend_window(): jnp.einsum('qhgd,khd->hgqk', queries.reshape(length, kv_here, grouping, H...  7.16 us
  transfers between devices with their start and end apart: 7, of which 4 were waited for; matrix products, arithmetic and copies ran while one was open for 18% of the time, Pallas kernels for 0%

commit v1 on v0

--- a/solution.py
+++ b/solution.py
@@ -161,7 +161,7 @@
         [hidden, shared_hidden.reshape(tokens_here // packing, units_here)], axis=0
     )
     columns = local_down.shape[1]
-    portion = lax.all_gather(stacked, "tp", axis=1, tiled=True)
+    portion = jnp.concatenate(lax.all_gather(stacked, "tp"), axis=1)
     shards_in = portion.shape[1] // units_here
     routed = jnp.dot(portion[:slots_all], local_down, preferred_element_type=jnp.float32)
     shared_piece = portion[slots_all:].reshape(

time: 299 us -> 304 us (1.017)
  local copies, waits for them, and re-layouts: 35.3 us -> 44.3 us
  matrix products: 34.9 us -> 31.5 us
    all_gather x0 -> x1, local copies, waits for them, and re-layouts: none -> 4.27 us  [shards(): portion = jnp.concatenate(lax.all_gather(stacked, 'tp'), axis=1)]
    dot_general x1, matrix products: 8.88 us -> 5.39 us  [shards(): jnp.dot(portion[:slots_all], local_down, preferred_element_type=jnp.float32)]
    unnamed x63 -> x68, local copies, waits for them, and re-layouts: 8.45 us -> 11.2 us
  transfers between devices with their start and end apart: 7 -> 7, of which waited for: 4 -> 4; matrix products, arithmetic and copies ran while one was open for 18% -> 19% of each run, Pallas kernels for 0% -> 0%
where the time goes in v1:
time: 304 us
  waiting for transfers between devices  174 us (57%)
  local copies, waits for them, and re-layouts  44.3 us (15%)
  matrix products  31.5 us (10%)
  other arithmetic  23.4 us (8%)
  starting transfers between devices  16.2 us (5%)
  between operations  14.4 us (5%)
    all_gather x1, waiting for transfers between devices, shards(): lax.all_gather(arrived, 'tp', axis=1, tiled=True)  77.6 us
    all_to_all x1, waiting for transfers between devices, shards(): lax.all_to_all(outgoing.reshape(ep_size, capacity, width_here), 'ep', spl...  45.4 us
    all_to_all x1, waiting for transfers between devices, shards(): lax.all_to_all(routed.astype(jnp.bfloat16).reshape(ep_size, capacity, col...  26.8 us
    all_gather x1, waiting for transfers between devices, shards(): portion = jnp.concatenate(lax.all_gather(stacked, 'tp'), axis=1)  23.2 us
    unnamed x68, local copies, waits for them, and re-layouts  11.2 us
    concatenate x4, local copies, waits for them, and re-layouts, rotate_heads(): jnp.concatenate([half_turn(row_half), half_turn(col_half)], axis=-1)  7.81 us
    dot_general x1, matrix products, attend_window(): jnp.einsum('qhgd,khd->hgqk', queries.reshape(length, kv_here, grouping, H...  7.16 us
    dot_general x2, matrix products, project(): up_sum = jnp.dot(weighted, up_rows, preferred_element_type=jnp.float32)  6.92 us
  transfers between devices with their start and end apart: 7, of which 4 were waited for; matrix products, arithmetic and copies ran while one was open for 19% of the time, Pallas kernels for 0%

profile of v1, /device:TPU:0, one launch (start us, length us, event | category | flops | bytes accessed | tf_op | source)
XLA Modules:
  0.0 303.6 jit_solution(5480694493810051660)
XLA Ops:
  7.2 0.9 copy.85
  8.3 1.4 reduce-window.6
  11.2 4.2 %gather_fusion = bf16[960,1024]{1,0:T(8,128)(2,1)S(1)} fusion(bf16[160,1024]{1,0:T(8,128)(2,1)S(1)} %copy-done.1, s32[1024]{0:T(1024)S(1)} %pad_clamp_fusion.1), kind=kCustom, calls=%fused_computation | custom fusion | bytes 3936000 | tf_op jit(solution)/shard_map/jit(_take)/gather | solution.py:138
  15.4 1.5 select_select_fusion
  16.9 6.4 %all-to-all-start = ((bf16[8,120,1024]{2,1,0:T(8,128)(2,1)}), bf16[8,120,1024]{2,1,0:T(8,128)(2,1)S(1)}, u32[]{:S(2)}, u32[]{:S(2)}) async-start(bf16[8,120,1024]{2,1,0:T(8,128)(2,1)} %select_select_fusion), calls=%async_computation | async-start | bytes 3932160 | tf_op jit(solution)/shard_map/all_to_all | solution.py:140
  23.3 0.7 all-gather.7.cloned.1.call-update
  24.0 45.4 %all-to-all-done = bf16[8,120,1024]{2,1,0:T(8,128)(2,1)S(1)} async-done(((bf16[8,120,1024]{2,1,0:T(8,128)(2,1)}), bf16[8,120,1024]{2,1,0:T(8,128)(2,1)S(1)}, u32[]{:S(2)}, u32[]{:S(2)}) %all-to-all-start) | async-done | bytes 1966112 | tf_op jit(solution)/shard_map/all_to_all | solution.py:140
  69.5 1.3 copy-done.7
  70.9 1.8 fusion.13
  72.8 2.1 fusion.34
  75.4 77.6 %all-gather.5.cloned.1.call-done = bf16[960,4096]{1,0:T(8,128)(2,1)} async-done(((bf16[960,1024]{1,0:T(8,128)(2,1)}), bf16[960,4096]{1,0:T(8,128)(2,1)}) %all-gather.5.cloned.1.call-update) | async-done | bytes 7864336 | tf_op jit(solution)/shard_map/all_gather | solution.py:149
  153.1 5.0 %fusion.1 = f32[960]{0:T(1024)S(1)} fusion(bf16[960,4096]{1,0:T(8,128)(2,1)} %all-gather.5.cloned.1.call-done), kind=kLoop, calls=%fused_computation.5 | loop fusion | flops 11795520 | bytes 7868160 | tf_op jit(solution)/shard_map/reduce_sum | solution.py:91
  158.5 6.4 %fusion.3 = f32[960,512]{1,0:T(8,128)S(1)} fusion(bf16[960,4096]{1,0:T(8,128)(2,1)S(1)} %copy-done.6, f32[4096]{0:T(1024)S(1)} %copy-done.29, bf16[1,4096,512]{2,1,0:T(8,128)(2,1)} %param.27), kind=kOutput, calls=%fused_computation.9 | convolution fusion | flops 4038328320 | bytes 14041088 | tf_op jit(solution)/shard_map/dot_general | solution.py:90
  165.0 4.6 %multiply_convert_fusion = bf16[960,512]{1,0:T(8,128)(2,1)S(1)} fusion(f32[960,512]{1,0:T(8,128)S(1)} %fusion.3, bf16[1,4096,512]{2,1,0:T(8,128)(2,1)S(1)} %copy-done.26, bf16[960,4096]{1,0:T(8,128)(2,1)S(1)} %copy-done.6, f32[4096]{0:T(1024)S(1)} %copy-done.29, f32[960]{0:T(1024)S(1)} %add_rsqrt_fusion.2), kind=kOutput, calls=%fused_computation.33 | convolution fusion | flops 4042260480 | bytes 15027968 | tf_op jit(solution)/shard_map/dot_general | solution.py:89
  169.6 1.0 pad_maximum_fusion.1
  171.6 1.2 fusion.57
  174.1 1.0 pad_maximum_fusion.3
  175.1 1.3 collective-permute-start.1
  176.4 3.7 %collective-permute-start = (bf16[2,128,512]{1,2,0:T(8,128)(2,1)}, bf16[2,128,512]{1,2,0:T(8,128)(2,1)}, u32[]{:S(2)}, u32[]{:S(2)}) collective-permute-start(bf16[2,128,512]{1,2,0:T(8,128)(2,1)} %get-tuple-element.18), channel_id=1, source_target_pairs={{0,4},{4,8},{8,12},{12,16},{16,20},{20,24},{24,28},{1,5},{5,9},{9,... | collective-permute-start | bytes 786440 | tf_op jit(solution)/shard_map/ppermute | solution.py:20
  180.1 1.5 copy.77
  181.6 4.1 %reshape.389 = f32[512,4,2,128]{3,2,1,0:T(2,128)} reshape(bf16[512,1024]{1,0:T(8,128)(2,1)} %param.16) | data formatting | bytes 3145728 | tf_op jit(solution)/shard_map/convert_element_type | solution.py:34
  186.9 2.0 copy.82
  188.9 1.9 copy.81
  190.9 1.9 copy.80
  192.8 1.9 copy.79
  194.8 0.6 add.209
  195.7 0.8 copy.91
  196.5 0.7 copy.93
  197.9 1.4 fusion.27
  199.3 23.2 %all-gather.9.cloned.1.call-done = bf16[4000,512]{1,0:T(8,128)(2,1)} async-done(((bf16[1000,512]{1,0:T(8,128)(2,1)}), bf16[4000,512]{1,0:T(8,128)(2,1)}) %all-gather.9.cloned.1.call-update) | async-done | bytes 4096016 | tf_op jit(solution)/shard_map/all_gather | solution.py:164
  222.5 4.3 %copy.118 = bf16[4,1000,512]{2,0,1:T(4,128)(2,1)S(1)} copy(bf16[4,1000,512]{2,1,0:T(8,128)(2,1)} %bitcast.111) | data formatting | bytes 8192000 | tf_op jit(solution)/shard_map/all_gather | solution.py:164
  226.8 1.4 slice.53
  228.7 1.3 copy.102
  230.0 0.9 copy-done.27
  230.9 5.4 %fusion.19 = bf16[960,1024]{1,0:T(8,128)(2,1)} fusion(bf16[960,2048]{1,0:T(8,128)(2,1)S(1)} %bitcast.112, bf16[1,2048,1024]{2,1,0:T(8,128)(2,1)S(1)} %copy-done.27), kind=kOutput, calls=%fused_computation.35 | convolution fusion | flops 4027514880 | bytes 10092544 | tf_op jit(solution)/shard_map/dot_general | solution.py:166
  236.3 4.7 %all-to-all-start.1 = ((bf16[8,120,1024]{2,1,0:T(8,128)(2,1)}), bf16[8,120,1024]{2,1,0:T(8,128)(2,1)S(1)}, u32[]{:S(2)}, u32[]{:S(2)}) async-start(bf16[8,120,1024]{2,1,0:T(8,128)(2,1)} %bitcast.118), calls=%async_computation.1 | async-start | bytes 3932160 | tf_op jit(solution)/shard_map/all_to_all | solution.py:172
  241.0 1.3 pad_clamp_fusion
  242.3 1.5 pad_maximum_fusion
  244.9 0.9 copy-done.3
  245.7 7.2 %fusion.2 = (f32[4,2,512]{2,1,0:T(2,128)S(1)}, f32[4,768,512,2]{2,1,3,0:T(8,128)S(1)}) fusion(pred[512,768]{0,1:T(8,128)(4,1)} %fusion.27, bf16[768,4,128,1]{0,2,3,1:T(8,128)(2,1)S(1)} %bitcast.113, f32[512,4,2,32]{3,0,2,1:T(8,128)S(1)} %copy-done.3, f32[512,4,2,32]{3,0,2,1:T(8,128)S(1)} %copy-done.4, f32[512,4,2,32]{3,0,2,1:T(8,128)S(1)} %copy-done.5, ...), kind=kOutput, calls=%fused_computation.8 | convolution fusion | flops 819458048 | bytes 18514432 | tf_op jit(solution)/shard_map/qhgd,khd->hgqk/dot_general | solution.py:71
  253.0 4.2 %fusion.28 = bf16[4,128,2,512]{3,1,2,0:T(8,128)(2,1)} fusion(bf16[768,4,128,1]{0,2,3,1:T(8,128)(2,1)S(1)} %bitcast.120, f32[4,768,512,2]{2,1,3,0:T(8,128)S(1)} %get-tuple-element.29, f32[4,2,512]{2,1,0:T(2,128)S(1)} %broadcast_add_fusion, pred[512,768]{0,1:T(8,128)(4,1)S(1)} %copy-done.13), kind=kOutput, calls=%fused_computation.40 | convolution fusion | flops 818413568 | bytes 14827520 | tf_op jit(solution)/shard_map/hgqk,khd->qhgd/dot_general | solution.py:82
  257.2 2.3 copy.95
  259.5 1.0 slice.52
  260.5 26.8 %all-to-all-done.1 = bf16[8,120,1024]{2,1,0:T(8,128)(2,1)S(1)} async-done(((bf16[8,120,1024]{2,1,0:T(8,128)(2,1)}), bf16[8,120,1024]{2,1,0:T(8,128)(2,1)S(1)}, u32[]{:S(2)}, u32[]{:S(2)}) %all-to-all-start.1) | async-done | bytes 1966112 | tf_op jit(solution)/shard_map/all_to_all | solution.py:172
  287.3 3.5 %gather_fusion.1 = bf16[640,1024]{1,0:T(8,128)(2,1)} fusion(bf16[960,1024]{1,0:T(8,128)(2,1)S(1)} %bitcast.101, s32[1024]{0:T(1024)S(1)} %copy-done.20), kind=kCustom, calls=%fused_computation.1 | custom fusion | bytes 2624000 | tf_op jit(solution)/shard_map/jit(_take)/gather | solution.py:180
  290.7 2.6 gather.15
  293.4 2.6 multiply_reduce_fusion
  296.0 1.1 fusion.29
  (119 shorter events, 8.8 us)
Async XLA Ops:
  7.2 288.8 %copy-start = (bf16[512,1024]{1,0:T(8,128)(2,1)S(1)}, bf16[512,1024]{1,0:T(8,128)(2,1)}, u32[]{:S(2)}) copy-start(bf16[512,1024]{1,0:T(8,128)(2,1)} %param.31) | copy-start | bytes 3145732
  7.2 4.0 %copy-start.1 = (bf16[160,1024]{1,0:T(8,128)(2,1)S(1)}, bf16[160,1024]{1,0:T(8,128)(2,1)}, u32[]{:S(2)}) copy-start(bf16[160,1024]{1,0:T(8,128)(2,1)} %param.22) | copy-start | bytes 983044
  16.9 52.6 %all-to-all-start = ((bf16[8,120,1024]{2,1,0:T(8,128)(2,1)}), bf16[8,120,1024]{2,1,0:T(8,128)(2,1)S(1)}, u32[]{:S(2)}, u32[]{:S(2)}) async-start(bf16[8,120,1024]{2,1,0:T(8,128)(2,1)} %select_select_fusion), calls=%async_computation | async-start | bytes 3932160 | tf_op jit(solution)/shard_map/all_to_all | solution.py:140
  23.3 49.5 %copy-start.29 = (f32[4096]{0:T(1024)S(1)}, f32[4096]{0:T(1024)}, u32[]{:S(2)}) copy-start(f32[4096]{0:T(1024)} %param.23) | copy-start | bytes 49156
  23.3 47.7 %all-gather.7.cloned.1.call-start = ((), (), s32[]{:S(2)}) async-start(), calls=%async_computation.3 | async-start | bytes 1638400 | tf_op jit(solution)/shard_map/all_gather | solution.py:152
  24.0 129.1 %all-gather.5.cloned.1.call-start = ((), (), s32[]{:S(2)}) async-start(), calls=%async_computation.2 | async-start | bytes 9830400 | tf_op jit(solution)/shard_map/all_gather | solution.py:149
  69.5 1.3 copy-start.7
  70.8 4.0 %copy-start.28 = (bf16[4096,128]{1,0:T(8,128)(2,1)S(1)}, bf16[4096,128]{1,0:T(8,128)(2,1)}, u32[]{:S(2)}) copy-start(bf16[4096,128]{1,0:T(8,128)(2,1)} %param.30) | copy-start | bytes 3145732
  70.9 151.7 %all-gather.9.cloned.1.call-start = ((), (), s32[]{:S(2)}) async-start(), calls=%async_computation.4 | async-start | bytes 5120000 | tf_op jit(solution)/shard_map/all_gather | solution.py:164
  70.9 4.0 %copy-start.14 = (bf16[160,4096]{1,0:T(8,128)(2,1)S(1)}, bf16[160,4096]{1,0:T(8,128)(2,1)}, u32[]{:S(2)}) copy-start(bf16[160,4096]{1,0:T(8,128)(2,1)} %all-gather.7.cloned.1.call-done) | copy-start | bytes 3932164
  153.1 5.5 %copy-start.6 = (bf16[960,4096]{1,0:T(8,128)(2,1)S(1)}, bf16[960,4096]{1,0:T(8,128)(2,1)}, u32[]{:S(2)}) copy-start(bf16[960,4096]{1,0:T(8,128)(2,1)} %all-gather.5.cloned.1.call-done) | copy-start | bytes 23592964
  158.5 6.4 %copy-start.26 = (bf16[1,4096,512]{2,1,0:T(8,128)(2,1)S(1)}, bf16[1,4096,512]{2,1,0:T(8,128)(2,1)}, u32[]{:S(2)}) copy-start(bf16[1,4096,512]{2,1,0:T(8,128)(2,1)} %param.26) | copy-start | bytes 12582916
  169.5 1.2 copy-start.15
  169.6 1.6 copy-start.16
  171.1 3.0 copy-start.8
  171.4 1.9 copy-start.25
  172.8 0.7 copy-start.11
  172.8 0.8 copy-start.12
  174.1 2.3 copy-start.10
  175.1 67.2 %collective-permute-start.1 = (bf16[2,128,512]{1,2,0:T(8,128)(2,1)}, bf16[2,128,512]{1,2,0:T(8,128)(2,1)}, u32[]{:S(2)}, u32[]{:S(2)}) collective-permute-start(bf16[2,128,512]{1,2,0:T(8,128)(2,1)} %get-tuple-element.19), channel_id=1, source_target_pairs={{4,0},{8,4},{12,8},{16,12},{20,16},{24,20},{28,24},{5,1},{9,5},{13... | collective-permute-start | bytes 786440 | tf_op jit(solution)/shard_map/ppermute | solution.py:23
  176.4 66.0 %collective-permute-start = (bf16[2,128,512]{1,2,0:T(8,128)(2,1)}, bf16[2,128,512]{1,2,0:T(8,128)(2,1)}, u32[]{:S(2)}, u32[]{:S(2)}) collective-permute-start(bf16[2,128,512]{1,2,0:T(8,128)(2,1)} %get-tuple-element.18), channel_id=1, source_target_pairs={{0,4},{4,8},{8,12},{12,16},{16,20},{20,24},{24,28},{1,5},{5,9},{9,... | collective-permute-start | bytes 786440 | tf_op jit(solution)/shard_map/ppermute | solution.py:20
  181.6 4.6 %copy-start.22 = (f32[128]{0:T(128)S(1)}, f32[128]{0:T(128)}, u32[]{:S(2)}) copy-start(f32[128]{0:T(128)} %param.19) | copy-start | bytes 1540
  190.9 3.9 %copy-start.30 = (f32[8]{0:T(128)S(1)}, f32[8]{0:T(128)}, u32[]{:S(2)}) copy-start(f32[8]{0:T(128)} %param.21) | copy-start | bytes 100
  190.9 4.5 %copy-start.19 = (s32[160,4]{0,1:T(4,128)S(1)}, s32[160,4]{0,1:T(4,128)}, u32[]{:S(2)}) copy-start(s32[160,4]{0,1:T(4,128)} %param.24) | copy-start | bytes 7684
  190.9 4.8 %copy-start.24 = (f32[160,4]{0,1:T(4,128)S(1)}, f32[160,4]{0,1:T(4,128)}, u32[]{:S(2)}) copy-start(f32[160,4]{0,1:T(4,128)} %param.25) | copy-start | bytes 7684
  226.8 1.9 copy-start.2
  228.7 2.2 copy-start.27
  236.3 6.0 %copy-start.9 = (bf16[512,512]{0,1:T(8,128)(2,1)S(1)}, bf16[512,512]{0,1:T(8,128)(2,1)}, u32[]{:S(2)}) copy-start(bf16[512,512]{0,1:T(8,128)(2,1)} %copy-done.8) | copy-start | bytes 1572868
  236.3 51.0 %all-to-all-start.1 = ((bf16[8,120,1024]{2,1,0:T(8,128)(2,1)}), bf16[8,120,1024]{2,1,0:T(8,128)(2,1)S(1)}, u32[]{:S(2)}, u32[]{:S(2)}) async-start(bf16[8,120,1024]{2,1,0:T(8,128)(2,1)} %bitcast.118), calls=%async_computation.1 | async-start | bytes 3932160 | tf_op jit(solution)/shard_map/all_to_all | solution.py:172
  242.3 1.9 copy-start.4
  242.3 2.5 copy-start.5
  243.8 1.9 copy-start.3
  243.8 1.9 copy-start.23
  245.7 7.2 %copy-start.21 = (f32[4,2]{1,0:T(4,128)S(1)}, f32[4,2]{1,0:T(4,128)}, u32[]{:S(2)}) copy-start(f32[4,2]{1,0:T(4,128)} %add.209) | copy-start | bytes 100
  245.7 7.3 %copy-start.13 = (pred[512,768]{0,1:T(8,128)(4,1)S(1)}, pred[512,768]{0,1:T(8,128)(4,1)}, u32[]{:S(2)}) copy-start(pred[512,768]{0,1:T(8,128)(4,1)} %fusion.27) | copy-start | bytes 1179652
  257.2 30.0 %copy-start.20 = (s32[1024]{0:T(1024)S(1)}, s32[1024]{0:T(1024)}, u32[]{:S(2)}) copy-start(s32[1024]{0:T(1024)} %pad_clamp_fusion) | copy-start | bytes 12292
  290.7 2.7 copy-start.17
  290.7 2.7 copy-start.18
Sparse Core Ops, SparseCore 0:
  25.9 30.1 all-gather.6
  71.0 82.0 all-gather.4
  170.7 51.7 all-gather.8
